TPU v7x, 32 devices: a whole 2x2x4 slice. The times are simulated.
32 devices in a mesh: ep: 16 (over z, y, core), tp: 2 (over x).
Axes of the slice: x: 2, y: 2, z: 4, core: 2. Of those that a mesh axis runs over, the one named last changes fastest.
Arguments:
- tokens: bfloat16 [256, 2048], P('ep'), may hold values from -6 to 6
- positions: int32 [256], P('ep'), may hold values from 1024 to 16383
- state: float32 [256, 4, 128, 128], P('ep', 'tp'), may hold values from -1 to 1
- mix_gain: float32 [2048], replicated, may hold values from 0.1 to 1.9
- w_query: bfloat16 [2048, 512], P(None, 'tp'), may hold values from -0.125 to 0.125
- w_key: bfloat16 [2048, 512], P(None, 'tp'), may hold values from -0.125 to 0.125
- w_value: bfloat16 [2048, 512], P(None, 'tp'), may hold values from -0.125 to 0.125
- w_out: bfloat16 [512, 2048], P('tp'), may hold values from -0.25 to 0.25
- ffn_gain: float32 [2048], replicated, may hold values from 0.1 to 1.9
- branch_gate: bfloat16 [2048], replicated, may hold values from -0.125 to 0.125
- dense_gate: bfloat16 [2048, 4096], P('tp', 'ep'), may hold values from -0.125 to 0.125
- dense_up: bfloat16 [2048, 4096], P('tp', 'ep'), may hold values from -0.125 to 0.125
- dense_down: bfloat16 [4096, 2048], P('ep', 'tp'), may hold values from -0.09375 to 0.09375
- routes: int32 [256, 6], P('ep'), may hold values from 0 to 15, all different within a row; in each aligned block of 16 rows (0 to 15, 16 to 31, ...) at most 12 rows name the same one
- route_scores: float32 [256, 6], P('ep'), may hold values from 0.05 to 1
- expert_gate: bfloat16 [16, 2048, 512], P('ep', None, 'tp'), may hold values from -0.125 to 0.125
- expert_up: bfloat16 [16, 2048, 512], P('ep', None, 'tp'), may hold values from -0.125 to 0.125
- expert_down: bfloat16 [16, 512, 2048], P('ep', 'tp'), may hold values from -0.25 to 0.25
Outputs:
- layer_out: bfloat16 [256, 2048], P('ep', 'tp')
Inputs may be any that keep to these rules, and one draw needn't show every extreme that they name: `routes`: each row names 6 different experts. In each aligned block of 16 rows (the rows of one index of ep) no expert is named by more than 12 rows, a bound that some block reaches.
All inputs are finite; a program needn't handle non-finite values.
Results may differ from a plain program's by a relative error of at most 0.012.
Values may be sent and summed in bfloat16 or wider, within the bound.
A program may use at most 64 MiB of HBM per device.

v0:
```python
import jax
import jax.numpy as jnp
from jax import lax
from jax.sharding import PartitionSpec as P

EPS = 1e-06


def normalize(inputs, scale_vec):
    values = inputs.astype(jnp.float32)
    return values * lax.rsqrt(jnp.mean(values * values, axis=-1, keepdims=True) + EPS) * scale_vec


def rotate(vectors, where):
    half = vectors.shape[-1] // 2
    inverse = 1.0 / 10000.0 ** jnp.linspace(0.0, 1.0, half, dtype=jnp.float32)
    angle = where.astype(jnp.float32)[:, None] * inverse[None, :]
    cosine = jnp.cos(angle)[:, None, :]
    sine = jnp.sin(angle)[:, None, :]
    first = vectors[..., :half]
    second = vectors[..., half:]
    return jnp.concatenate(
        [first * cosine - second * sine, second * cosine + first * sine], axis=-1
    )


def on_device(
    tokens,
    positions,
    state,
    mix_gain,
    w_query,
    w_key,
    w_value,
    w_out,
    ffn_gain,
    branch_gate,
    dense_gate,
    dense_up,
    dense_down,
    routes,
    route_scores,
    expert_gate,
    expert_up,
    expert_down,
):
    sequences = tokens.shape[0]
    model_width = tokens.shape[1]
    tp_count = lax.axis_size("tp")
    ep_count = lax.axis_size("ep")
    columns = model_width // tp_count
    tp_index = lax.axis_index("tp")
    local_heads = state.shape[1]
    head_dim = state.shape[2]
    normed = normalize(tokens, mix_gain).astype(jnp.bfloat16)
    query_vec = jnp.dot(normed, w_query, preferred_element_type=jnp.float32).reshape(
        sequences, local_heads, head_dim
    )
    key_vec = jnp.dot(normed, w_key, preferred_element_type=jnp.float32).reshape(
        sequences, local_heads, head_dim
    )
    value_vec = jnp.dot(normed, w_value, preferred_element_type=jnp.float32).reshape(
        sequences, local_heads, head_dim
    )
    query_vec = rotate(query_vec, positions)
    key_vec = rotate(key_vec, positions) * head_dim ** (-0.5)
    all_heads = local_heads * tp_count
    head_index = (tp_index * local_heads + jnp.arange(local_heads, dtype=jnp.int32)).astype(
        jnp.float32
    )
    decay_rate = 1.0 - 2.0 ** (-5.0 - 5.0 * head_index / (all_heads - 1))
    new_state = (
        decay_rate[None, :, None, None] * state + key_vec[:, :, :, None] * value_vec[:, :, None, :]
    )
    retrieved = jnp.einsum("bhd,bhde->bhe", query_vec, new_state, precision=lax.Precision.HIGHEST)
    retrieved = retrieved * lax.rsqrt(jnp.mean(retrieved * retrieved, axis=-1, keepdims=True) + EPS)
    retrieved = retrieved.reshape(sequences, local_heads * head_dim).astype(jnp.bfloat16)
    head_partial = jnp.dot(retrieved, w_out, preferred_element_type=jnp.float32).astype(
        jnp.bfloat16
    )
    mixer_out = lax.psum(head_partial.astype(jnp.float32).astype(jnp.bfloat16), "tp").astype(
        jnp.float32
    )
    after_mix = tokens.astype(jnp.float32) + mixer_out
    ffn_in = normalize(after_mix, ffn_gain).astype(jnp.bfloat16)
    own_cols = lax.dynamic_slice_in_dim(ffn_in, tp_index * columns, columns, 1)
    per_device = expert_gate.shape[0]
    experts = per_device * ep_count
    fanout = routes.shape[1]
    capacity = max(2, min(sequences, 2 * sequences * fanout // experts))
    slot_count = experts * capacity
    marks = (routes[:, :, None] == jnp.arange(experts, dtype=jnp.int32)[None, None, :]).astype(
        jnp.int32
    )
    flattened = marks.reshape(sequences * fanout, experts)
    ranking = jnp.sum((jnp.cumsum(flattened, axis=0) - flattened) * flattened, axis=1).reshape(
        sequences, fanout
    )
    slot_index = routes * capacity + ranking
    matches = jnp.arange(slot_count, dtype=jnp.int32)[:, None, None] == slot_index[None]
    placing = jnp.any(matches, axis=2).astype(jnp.bfloat16)
    route_weights = route_scores / jnp.sum(route_scores, axis=1, keepdims=True)
    combining = jnp.sum(jnp.where(matches, route_weights[None], 0.0), axis=2).T
    packed = jnp.dot(placing, own_cols, preferred_element_type=jnp.float32).astype(jnp.bfloat16)
    packed = packed.reshape(experts, capacity, own_cols.shape[1])
    received = lax.all_to_all(packed, "ep", split_axis=0, concat_axis=0, tiled=True)
    received = lax.all_gather(received, "tp", axis=2, tiled=True)
    count = received.shape[1]
    grouped = received.reshape(ep_count, per_device, count, model_width)
    gate_pre = jnp.einsum(
        "skcd,kdw->skcw", grouped, expert_gate, preferred_element_type=jnp.float32
    )
    up_pre = jnp.einsum("skcd,kdw->skcw", grouped, expert_up, preferred_element_type=jnp.float32)
    hidden = (jax.nn.silu(gate_pre) * up_pre).astype(jnp.bfloat16)
    partial_out = jnp.einsum(
        "skcw,kwd->skcd", hidden, expert_down, preferred_element_type=jnp.float32
    )
    blocks_out = partial_out.astype(jnp.bfloat16).reshape(
        ep_count, per_device, count, tp_count, columns
    )
    traded = lax.all_to_all(blocks_out, "tp", split_axis=3, concat_axis=3, tiled=True)
    mine = jnp.sum(traded.astype(jnp.float32), axis=3).astype(jnp.bfloat16)
    mine = mine.reshape(ep_count * per_device, count, columns)
    returned = lax.all_to_all(mine, "ep", split_axis=0, concat_axis=0, tiled=True)
    experts_out = jnp.dot(
        combining,
        returned.reshape(slot_count, columns).astype(jnp.float32),
        precision=lax.Precision.HIGHEST,
    )
    hidden_units = dense_gate.shape[1]
    both_weights = jnp.concatenate([dense_gate, dense_up], axis=1)
    pre_parts = jnp.dot(
        lax.all_gather(own_cols, "ep", axis=0, tiled=True),
        both_weights,
        preferred_element_type=jnp.float32,
    ).astype(jnp.bfloat16)
    pre_total = lax.psum(pre_parts.astype(jnp.float32).astype(jnp.bfloat16), "tp").astype(
        jnp.float32
    )
    dense_hidden = (jax.nn.silu(pre_total[:, :hidden_units]) * pre_total[:, hidden_units:]).astype(
        jnp.bfloat16
    )
    dense_out = lax.psum_scatter(
        jnp.dot(dense_hidden, dense_down, preferred_element_type=jnp.float32),
        "ep",
        scatter_dimension=0,
        tiled=True,
    )
    branch_weight = jax.nn.sigmoid(jnp.dot(ffn_in, branch_gate, preferred_element_type=jnp.float32))
    residual_cols = lax.dynamic_slice_in_dim(after_mix, tp_index * columns, columns, 1)
    layer_out = residual_cols + experts_out + branch_weight[:, None] * dense_out
    return layer_out.astype(jnp.bfloat16)


def solution(mesh):
    placed = (
        P("ep", None),
        P("ep"),
        P("ep", "tp", None, None),
        P(),
        P(None, "tp"),
        P(None, "tp"),
        P(None, "tp"),
        P("tp", None),
        P(),
        P(),
        P("tp", "ep"),
        P("tp", "ep"),
        P("ep", "tp"),
        P("ep", None),
        P("ep", None),
        P("ep", None, "tp"),
        P("ep", None, "tp"),
        P("ep", "tp", None),
    )
    return jax.shard_map(
        on_device, mesh=mesh, in_specs=placed, out_specs=P("ep", "tp"), check_vma=False
    )
```

profile of v0, /device:TPU:0, one launch (start us, length us, event | category | flops | bytes accessed | tf_op | source)
XLA Modules:
  0.0 169.2 jit_solution(17816289287856958037)
XLA Ops:
  6.5 0.0 copy-start
  6.5 0.0 all-reduce.3.cloned.1.call-start
  6.6 0.8 convert_element_type.77
  7.4 1.0 fusion.30
  8.5 1.6 fusion.47
  10.1 1.6 fusion.45
  11.6 0.0 copy-done.1
  11.7 0.0 copy-done.7
  11.7 1.5 fusion.49
  13.2 0.0 copy-start.3
  13.2 0.1 fusion.41
  13.3 0.1 multiply_cosine_fusion
  13.4 0.0 copy-start.10
  13.4 0.1 multiply_subtract_fusion
  13.5 0.1 pad_maximum_fusion
  13.7 2.1 %fusion = f32[16,2,1,128]{3,2,1,0:T(1,128)S(1)} fusion(f32[16,2,128,1]{2,3,1,0:T(1,128)S(1)} %bitcast.86, f32[16,2,128,128]{3,2,1,0:T(8,128)S(1)} %copy-done.2, f32[16,2,128]{2,1,0:T(2,128)S(1)} %mul.244, f32[16,2,128]{2,1,0:T(2,128)S(1)} %get-tuple-element.17, f32[2]{0:T(128)S(1)} %power_subtract_fusion), kind=kOutput, calls=%fused_computation.2 | convolution fusion | flops 7864320 | bytes 2162696 | tf_op jit(solution)/shard_map/bhd,bhde->bhe/dot_general | solution.py:75
  15.7 0.1 multiply_reduce_fusion.1
  15.8 0.1 multiply_convert_fusion.1
  15.9 0.0 copy-done.3
  15.9 0.9 convolution_convert_fusion.1
  16.8 0.0 all-reduce.3.cloned.1.call-update
  16.9 0.1 copy.59
  16.9 0.1 eq.30
  17.0 0.1 fusion.38
  17.1 0.1 reduce_window_sum.11
  17.3 0.2 select_reduce_fusion.1
  17.4 0.1 reshape.154
  17.5 0.1 copy.60
  17.6 0.1 fusion.37
  17.7 23.0 %all-reduce.3.cloned.1.call-done = bf16[16,2048]{1,0:T(8,128)(2,1)} async-done(((bf16[16,2048]{1,0:T(8,128)(2,1)}), bf16[16,2048]{1,0:T(8,128)(2,1)}) %all-reduce.3.cloned.1.call-update) | async-done | bytes 65552 | tf_op jit(solution)/shard_map/psum | solution.py:81
  40.7 1.6 convert_add_fusion
  42.3 0.9 multiply_convert_fusion
  43.3 22.9 %all_gather.7 = bf16[256,1024]{1,0:T(8,128)(2,1)S(1)} all-gather(bf16[16,1024]{1,0:T(8,128)(2,1)S(1)} %constant_dynamic-slice_fusion), channel_id=1, replica_groups=mesh['ep'=16,'tp'=2] {'ep'}, dimensions={0}, use_global_device_ids=true | all-gather | bytes 557056 | tf_op jit(solution)/shard_map/all_gather | solution.py:133
  66.2 0.3 convolution_convert_fusion.2
  66.5 0.9 reshape.155
  67.4 3.6 %all-to-all-start = ((bf16[16,12,1024]{2,1,0:T(8,128)(2,1)}), bf16[16,12,1024]{2,1,0:T(8,128)(2,1)S(1)}, u32[]{:S(2)}, u32[]{:S(2)}) async-start(bf16[16,12,1024]{2,1,0:T(8,128)(2,1)} %reshape.155), calls=%async_computation | async-start | bytes 1048576 | tf_op jit(solution)/shard_map/all_to_all | solution.py:106
  70.9 0.0 copy-start.5
  71.0 0.0 all-reduce.5.cloned.1.call-start
  71.0 2.2 %convolution_convert_fusion.3 = bf16[256,512]{1,0:T(8,128)(2,1)} fusion(bf16[256,1024]{1,0:T(8,128)(2,1)S(1)} %all_gather.7, bf16[1024,256]{1,0:T(8,128)(2,1)S(1)} %copy-done.12, bf16[1024,256]{1,0:T(8,128)(2,1)} %param.30), kind=kOutput, calls=%fused_computation.7 | convolution fusion | flops 270663680 | bytes 1835008 | tf_op jit(solution)/shard_map/dot_general | solution.py:132
  73.2 0.0 all-reduce.5.cloned.1.call-update
  73.3 0.0 reduce-scatter.2.cloned.1.call-start
  73.3 24.4 %all-reduce.5.cloned.1.call-done = bf16[256,512]{1,0:T(8,128)(2,1)} async-done(((bf16[256,512]{1,0:T(8,128)(2,1)}), bf16[256,512]{1,0:T(8,128)(2,1)}) %all-reduce.5.cloned.1.call-update) | async-done | bytes 262160 | tf_op jit(solution)/shard_map/psum | solution.py:137
  97.7 1.0 convert_element_type.92
  98.8 0.0 copy-start.4
  98.8 1.3 fusion.33
  100.1 0.0 reduce-scatter.2.cloned.1.call-update
  100.1 0.0 all-to-all-done
  100.1 0.2 copy.61
  100.3 11.0 %all_gather.6 = bf16[16,12,2048]{2,0,1:T(8,128)(2,1)S(1)} all-gather(bf16[16,12,1024]{2,0,1:T(8,128)(2,1)S(1)} %copy.61), channel_id=1, replica_groups=mesh['ep'=16,'tp'=2] {'tp'}, dimensions={2}, use_global_device_ids=true | all-gather | bytes 1179648 | tf_op jit(solution)/shard_map/all_gather | solution.py:107
  111.4 1.1 convolution_bitcast_fusion.1
  112.4 2.3 %convolution_convert_fusion = bf16[16,12,2048]{2,0,1:T(8,128)(2,1)S(1)} fusion(bf16[1,256,2048]{2,1,0:T(8,128)(2,1)S(1)} %copy-done, bf16[16,12,2048]{2,0,1:T(8,128)(2,1)S(1)} %all_gather.6, bf16[1,2048,256]{2,1,0:T(8,128)(2,1)} %param.36, f32[16,1,12,256]{3,0,2,1:T(8,128)} %convolution_bitcast_fusion.1), kind=kOutput, calls=%fused_computation | convolution fusion | flops 403341312 | bytes 3866624 | tf_op jit(solution)/shard_map/skcw,kwd->skcd/dot_general | solution.py:115
  114.7 0.1 copy.77
  114.8 0.0 copy-start.11
  114.8 0.0 copy-start.9
  114.8 12.1 %all_to_all.15 = bf16[16,1,12,2,1024]{4,0,2,1,3:T(8,128)(2,1)S(1)} all-to-all(bf16[16,1,12,2,1024]{4,0,2,1,3:T(8,128)(2,1)S(1)} %bitcast.82), channel_id=1, replica_groups=mesh['ep'=16,'tp'=2] {'tp'}, dimensions={3} | all-to-all | bytes 1572864 | tf_op jit(solution)/shard_map/all_to_all | solution.py:121
  126.9 0.2 reduce_sum.72
  127.1 1.0 copy.64
  128.2 5.6 %all-to-all-start.2 = ((bf16[16,12,1024]{2,1,0:T(8,128)(2,1)}), bf16[16,12,1024]{2,1,0:T(8,128)(2,1)S(1)}, u32[]{:S(2)}, u32[]{:S(2)}) async-start(bf16[16,12,1024]{2,1,0:T(8,128)(2,1)} %copy.64), calls=%async_computation.2 | async-start | bytes 1048576 | tf_op jit(solution)/shard_map/all_to_all | solution.py:124
  133.9 0.1 select_reduce_fusion
  134.0 0.1 fusion.12
  134.1 14.8 %all-to-all-done.2 = bf16[16,12,1024]{2,1,0:T(8,128)(2,1)S(1)} async-done(((bf16[16,12,1024]{2,1,0:T(8,128)(2,1)}), bf16[16,12,1024]{2,1,0:T(8,128)(2,1)S(1)}, u32[]{:S(2)}, u32[]{:S(2)}) %all-to-all-start.2) | async-done | bytes 393248 | tf_op jit(solution)/shard_map/all_to_all | solution.py:124
  148.9 0.1 reshape.161
  149.0 11.9 %reduce-scatter.2.cloned.1.call-done = f32[16,1024]{1,0:T(8,128)} async-done(((f32[256,1024]{1,0:T(8,128)}), f32[16,1024]{1,0:T(8,128)}) %reduce-scatter.2.cloned.1.call-update) | async-done | bytes 65552 | tf_op jit(solution)/shard_map/reduce_scatter | solution.py:143
  160.9 1.7 %fusion.8 = bf16[16,1024]{1,0:T(8,128)(2,1)} fusion(f32[192,16]{0,1:T(8,128)S(1)} %select_reduce_fusion, bf16[192,1024]{1,0:T(8,128)(2,1)S(1)} %reshape.161, f32[16,1024]{1,0:T(8,128)} %reduce-scatter.2.cloned.1.call-done, f32[16,2048]{1,0:T(8,128)S(1)} %copy-done.6, s32[]{:T(128)S(6)} %select_n.8, f32[16]{0:T(128)S(1)} %fusion.12), kind=kOutput, calls=%fused_computation.15 | convolution fusion | flops 37814272 | bytes 569412 | tf_op jit(solution)/shard_map/dot_general | solution.py:125
  (29 shorter events, 0.2 us)
Async XLA Ops:
  6.5 105.9 %copy-start = (bf16[1,256,2048]{2,1,0:T(8,128)(2,1)S(1)}, bf16[1,256,2048]{2,1,0:T(8,128)(2,1)}, u32[]{:S(2)}) copy-start(bf16[1,256,2048]{2,1,0:T(8,128)(2,1)} %param.37) | copy-start | bytes 3145732
  6.5 5.1 %copy-start.1 = (bf16[16,2048]{1,0:T(8,128)(2,1)S(1)}, bf16[16,2048]{1,0:T(8,128)(2,1)}, u32[]{:S(2)}) copy-start(bf16[16,2048]{1,0:T(8,128)(2,1)} %param.20) | copy-start | bytes 196612
  6.5 5.1 %copy-start.7 = (f32[2048]{0:T(1024)S(1)}, f32[2048]{0:T(1024)}, u32[]{:S(2)}) copy-start(f32[2048]{0:T(1024)} %param.23) | copy-start | bytes 24580
  6.5 7.1 %copy-start.2 = (f32[16,2,128,128]{3,2,1,0:T(8,128)S(1)}, f32[16,2,128,128]{3,2,1,0:T(8,128)}, u32[]{:S(2)}) copy-start(f32[16,2,128,128]{3,2,1,0:T(8,128)} %param.22) | copy-start | bytes 6291460
  6.5 34.1 %all-reduce.3.cloned.1.call-start = ((), (), s32[]{:S(2)}) async-start(), calls=%async_computation.4 | async-start | bytes 131072 | tf_op jit(solution)/shard_map/psum | solution.py:81
  13.2 3.7 %copy-start.8 = (s32[16,6]{0,1:T(8,128)S(1)}, s32[16,6]{0,1:T(8,128)}, u32[]{:S(2)}) copy-start(s32[16,6]{0,1:T(8,128)} %param.33) | copy-start | bytes 1156
  13.2 2.7 %copy-start.3 = (bf16[256,2048]{1,0:T(8,128)(2,1)S(1)}, bf16[256,2048]{1,0:T(8,128)(2,1)}, u32[]{:S(2)}) copy-start(bf16[256,2048]{1,0:T(8,128)(2,1)} %param.27) | copy-start | bytes 3145732
  13.4 28.9 %copy-start.10 = (f32[2048]{0:T(1024)S(1)}, f32[2048]{0:T(1024)}, u32[]{:S(2)}) copy-start(f32[2048]{0:T(1024)} %param.28) | copy-start | bytes 24580
  16.8 54.2 %copy-start.12 = (bf16[1024,256]{1,0:T(8,128)(2,1)S(1)}, bf16[1024,256]{1,0:T(8,128)(2,1)}, u32[]{:S(2)}) copy-start(bf16[1024,256]{1,0:T(8,128)(2,1)} %param.31) | copy-start | bytes 1572868
  67.4 32.7 %all-to-all-start = ((bf16[16,12,1024]{2,1,0:T(8,128)(2,1)}), bf16[16,12,1024]{2,1,0:T(8,128)(2,1)S(1)}, u32[]{:S(2)}, u32[]{:S(2)}) async-start(bf16[16,12,1024]{2,1,0:T(8,128)(2,1)} %reshape.155), calls=%async_computation | async-start | bytes 1048576 | tf_op jit(solution)/shard_map/all_to_all | solution.py:106
  70.9 27.8 %copy-start.5 = (bf16[256,1024]{1,0:T(8,128)(2,1)S(1)}, bf16[256,1024]{1,0:T(8,128)(2,1)}, u32[]{:S(2)}) copy-start(bf16[256,1024]{1,0:T(8,128)(2,1)} %param.32) | copy-start | bytes 1572868
  71.0 26.8 %all-reduce.5.cloned.1.call-start = ((), (), s32[]{:S(2)}) async-start(), calls=%async_computation.5 | async-start | bytes 524288 | tf_op jit(solution)/shard_map/psum | solution.py:137
  73.3 87.6 %reduce-scatter.2.cloned.1.call-start = ((), (), s32[]{:S(2)}) async-start(), calls=%async_computation.6 | async-start | bytes 1114112 | tf_op jit(solution)/shard_map/reduce_scatter | solution.py:143
  98.8 12.6 %copy-start.4 = (bf16[1,2048,256]{2,1,0:T(8,128)(2,1)S(1)}, bf16[1,2048,256]{2,1,0:T(8,128)(2,1)}, u32[]{:S(2)}) copy-start(bf16[1,2048,256]{2,1,0:T(8,128)(2,1)} %param.35) | copy-start | bytes 3145732
  114.8 19.0 %copy-start.11 = (bf16[2048]{0:T(1024)(128)(2,1)S(1)}, bf16[2048]{0:T(1024)(128)(2,1)}, u32[]{:S(2)}) copy-start(bf16[2048]{0:T(1024)(128)(2,1)} %param.29) | copy-start | bytes 12292
  114.8 19.0 %copy-start.9 = (f32[16,6]{0,1:T(8,128)S(1)}, f32[16,6]{0,1:T(8,128)}, u32[]{:S(2)}) copy-start(f32[16,6]{0,1:T(8,128)} %param.34) | copy-start | bytes 1156
  126.9 34.0 %copy-start.6 = (f32[16,2048]{1,0:T(8,128)S(1)}, f32[16,2048]{1,0:T(8,128)}, u32[]{:S(2)}) copy-start(f32[16,2048]{1,0:T(8,128)} %get-tuple-element.6) | copy-start | bytes 393220
  128.2 20.7 %all-to-all-start.2 = ((bf16[16,12,1024]{2,1,0:T(8,128)(2,1)}), bf16[16,12,1024]{2,1,0:T(8,128)(2,1)S(1)}, u32[]{:S(2)}, u32[]{:S(2)}) async-start(bf16[16,12,1024]{2,1,0:T(8,128)(2,1)} %copy.64), calls=%async_computation.2 | async-start | bytes 1048576 | tf_op jit(solution)/shard_map/all_to_all | solution.py:124
Sparse Core Ops, SparseCore 0:
  17.0 23.6 all-reduce.2
  74.0 23.6 all-reduce.4
  101.4 59.4 reduce-scatter.1
where the time goes:
time: 170 us; the launch traced here: 169 us
  waiting for transfers between devices  74.1 us (44%)
  blocking collectives  46 us (27%)
  matrix products  16.6 us (10%)
  between operations  13.5 us (8%)
  starting transfers between devices  9.31 us (5%)
  other arithmetic  6.78 us (4%)
  local copies, waits for them, and re-layouts  2.79 us (2%)
    psum x1, waiting for transfers between devices, on_device(): lax.psum(pre_parts.astype(jnp.float32).astype(jnp.bfloat16), 'tp')  24.4 us
    psum x1, waiting for transfers between devices, on_device(): lax.psum(head_partial.astype(jnp.float32).astype(jnp.bfloat16), 'tp')  23 us
    all_gather x1, blocking collectives, on_device(): lax.all_gather(own_cols, 'ep', axis=0, tiled=True)  22.9 us
    all_to_all x1, waiting for transfers between devices, on_device(): lax.all_to_all(mine, 'ep', split_axis=0, concat_axis=0, tiled=True)  14.8 us
    all_to_all x1, blocking collectives, on_device(): lax.all_to_all(blocks_out, 'tp', split_axis=3, concat_axis=3, tiled=True)  12.1 us
    reduce_scatter x1, waiting for transfers between devices, on_device(): lax.psum_scatter(jnp.dot(dense_hidden, dense_down, preferred_element_type...  11.9 us
    all_gather x1, blocking collectives, on_device(): received = lax.all_gather(received, 'tp', axis=2, tiled=True)  11 us
    all_to_all x1, starting transfers between devices, on_device(): lax.all_to_all(mine, 'ep', split_axis=0, concat_axis=0, tiled=True)  5.62 us
  transfers between devices with their start and end apart: 5, of which 4 were waited for; matrix products, arithmetic and copies ran while one was open for 6% of the time, Pallas kernels for 0%

commit v1 on v0

--- a/solution.py
+++ b/solution.py
@@ -134,9 +134,9 @@
         both_weights,
         preferred_element_type=jnp.float32,
     ).astype(jnp.bfloat16)
-    pre_total = lax.psum(pre_parts.astype(jnp.float32).astype(jnp.bfloat16), "tp").astype(
-        jnp.float32
-    )
+    pre_total = jnp.sum(
+        lax.all_gather(pre_parts.astype(jnp.float32).astype(jnp.bfloat16), "tp"), axis=0
+    ).astype(jnp.float32)
     dense_hidden = (jax.nn.silu(pre_total[:, :hidden_units]) * pre_total[:, hidden_units:]).astype(
         jnp.bfloat16
     )

time: 170 us -> 157 us (0.924)
  waiting for transfers between devices: 74.1 us -> 48.4 us
  blocking collectives: 46 us -> 59.7 us
    psum x1 -> x0, waiting for transfers between devices: 24.4 us -> none  [on_device(): lax.psum(pre_parts.astype(jnp.float32).astype(jnp.bfloat16), 'tp')]
    all_gather x0 -> x1, blocking collectives: none -> 9.22 us  [on_device(): lax.all_gather(pre_parts.astype(jnp.float32).astype(jnp.bfloat16), 'tp')]
    all_gather x1, blocking collectives: 22.9 us -> 26.9 us  [on_device(): lax.all_gather(own_cols, 'ep', axis=0, tiled=True)]
    all_to_all x1, starting transfers between devices: 3.57 us -> 5.62 us  [on_device(): lax.all_to_all(packed, 'ep', split_axis=0, concat_axis=0, tiled=True)]
    all_to_all x1, starting transfers between devices: 5.62 us -> 3.57 us  [on_device(): lax.all_to_all(mine, 'ep', split_axis=0, concat_axis=0, tiled=True)]
  transfers between devices with their start and end apart: 5 -> 4, of which waited for: 4 -> 3; matrix products, arithmetic and copies ran while one was open for 6% -> 6% of each run, Pallas kernels for 0% -> 0%
where the time goes in v1:
time: 157 us; the launch traced here: 156 us
  blocking collectives  59.7 us (38%)
  waiting for transfers between devices  48.4 us (31%)
  matrix products  16.1 us (10%)
  between operations  13.8 us (9%)
  starting transfers between devices  9.27 us (6%)
  other arithmetic  5.93 us (4%)
  local copies, waits for them, and re-layouts  2.79 us (2%)
    all_gather x1, blocking collectives, on_device(): lax.all_gather(own_cols, 'ep', axis=0, tiled=True)  26.9 us
    psum x1, waiting for transfers between devices, on_device(): lax.psum(head_partial.astype(jnp.float32).astype(jnp.bfloat16), 'tp')  23 us
    all_to_all x1, waiting for transfers between devices, on_device(): lax.all_to_all(mine, 'ep', split_axis=0, concat_axis=0, tiled=True)  14.3 us
    all_to_all x1, blocking collectives, on_device(): lax.all_to_all(blocks_out, 'tp', split_axis=3, concat_axis=3, tiled=True)  12.4 us
    all_gather x1, blocking collectives, on_device(): received = lax.all_gather(received, 'tp', axis=2, tiled=True)  11.2 us
    reduce_scatter x1, waiting for transfers between devices, on_device(): lax.psum_scatter(jnp.dot(dense_hidden, dense_down, preferred_element_type...  11.1 us
    all_gather x1, blocking collectives, on_device(): lax.all_gather(pre_parts.astype(jnp.float32).astype(jnp.bfloat16), 'tp')  9.22 us
    all_to_all x1, starting transfers between devices, on_device(): lax.all_to_all(packed, 'ep', split_axis=0, concat_axis=0, tiled=True)  5.62 us
  transfers between devices with their start and end apart: 4, of which 3 were waited for; matrix products, arithmetic and copies ran while one was open for 6% of the time, Pallas kernels for 0%

profile of v1, /device:TPU:0, one launch (start us, length us, event | category | flops | bytes accessed | tf_op | source)
XLA Modules:
  0.0 155.9 jit_solution(6780330245404084669)
XLA Ops:
  6.5 0.0 copy-start
  6.5 0.0 all-reduce.2.cloned.1.call-start
  6.6 0.8 convert_element_type.79
  7.4 1.0 fusion.30
  8.5 1.6 %fusion.47 = f32[16,256]{1,0:T(8,128)S(1)} fusion(bf16[2048,256]{1,0:T(8,128)(2,1)} %param.25, bf16[16,2048]{1,0:T(8,128)(2,1)} %param.20, f32[2048]{0:T(1024)} %param.23, f32[16]{0:T(128)S(1)} %add_rsqrt_fusion.2), kind=kOutput, calls=%fused_computation.81 | convolution fusion | flops 16908288 | bytes 1138752 | tf_op jit(solution)/shard_map/dot_general | solution.py:59
  10.1 1.6 %fusion.45 = f32[16,256]{1,0:T(8,128)S(1)} fusion(bf16[2048,256]{1,0:T(8,128)(2,1)} %param.26, bf16[16,2048]{1,0:T(8,128)(2,1)} %param.20, f32[2048]{0:T(1024)} %param.23, f32[16]{0:T(128)S(1)} %add_rsqrt_fusion.2), kind=kOutput, calls=%fused_computation.80 | convolution fusion | flops 16908288 | bytes 1138752 | tf_op jit(solution)/shard_map/dot_general | solution.py:62
  11.6 0.0 copy-done.1
  11.7 0.0 copy-done.7
  11.7 1.5 fusion.49
  13.2 0.0 copy-start.3
  13.2 0.1 fusion.41
  13.3 0.1 multiply_cosine_fusion
  13.4 0.0 copy-start.10
  13.4 0.1 multiply_subtract_fusion
  13.5 0.1 pad_maximum_fusion
  13.6 0.0 copy-done.2
  13.7 2.1 %fusion = f32[16,2,1,128]{3,2,1,0:T(1,128)S(1)} fusion(f32[16,2,128,1]{2,3,1,0:T(1,128)S(1)} %bitcast.88, f32[16,2,128,128]{3,2,1,0:T(8,128)S(1)} %copy-done.2, f32[16,2,128]{2,1,0:T(2,128)S(1)} %mul.244, f32[16,2,128]{2,1,0:T(2,128)S(1)} %get-tuple-element.17, f32[2]{0:T(128)S(1)} %power_subtract_fusion), kind=kOutput, calls=%fused_computation.2 | convolution fusion | flops 7864320 | bytes 2162696 | tf_op jit(solution)/shard_map/bhd,bhde->bhe/dot_general | solution.py:75
  15.7 0.1 multiply_reduce_fusion.1
  15.8 0.1 multiply_convert_fusion.1
  15.9 0.0 copy-done.3
  15.9 0.9 convolution_convert_fusion.1
  16.8 0.0 all-reduce.2.cloned.1.call-update
  16.9 0.1 copy.59
  16.9 0.1 eq.30
  17.0 0.1 fusion.38
  17.1 0.1 reduce_window_sum.11
  17.3 0.2 select_reduce_fusion.1
  17.4 0.1 reshape.154
  17.5 0.1 copy.60
  17.6 0.1 fusion.37
  17.7 23.0 %all-reduce.2.cloned.1.call-done = bf16[16,2048]{1,0:T(8,128)(2,1)} async-done(((bf16[16,2048]{1,0:T(8,128)(2,1)}), bf16[16,2048]{1,0:T(8,128)(2,1)}) %all-reduce.2.cloned.1.call-update) | async-done | bytes 65552 | tf_op jit(solution)/shard_map/psum | solution.py:81
  40.7 1.6 %convert_add_fusion = (f32[16,2048]{1,0:T(8,128)}, f32[16]{0:T(128)S(1)}) fusion(bf16[16,2048]{1,0:T(8,128)(2,1)S(1)} %copy-done.1, bf16[16,2048]{1,0:T(8,128)(2,1)} %all-reduce.2.cloned.1.call-done), kind=kLoop, calls=%fused_computation.38 | loop fusion | flops 163824 | bytes 262208 | tf_op jit(solution)/shard_map/add | solution.py:84
  42.3 0.9 multiply_convert_fusion
  43.3 0.3 convolution_convert_fusion.2
  43.6 0.9 reshape.155
  44.5 5.6 %all-to-all-start = ((bf16[16,12,1024]{2,1,0:T(8,128)(2,1)}), bf16[16,12,1024]{2,1,0:T(8,128)(2,1)S(1)}, u32[]{:S(2)}, u32[]{:S(2)}) async-start(bf16[16,12,1024]{2,1,0:T(8,128)(2,1)} %reshape.155), calls=%async_computation | async-start | bytes 1048576 | tf_op jit(solution)/shard_map/all_to_all | solution.py:106
  50.1 0.0 reduce-scatter.2.cloned.1.call-start
  50.1 26.9 %all_gather.13 = bf16[256,1024]{1,0:T(8,128)(2,1)S(1)} all-gather(bf16[16,1024]{1,0:T(8,128)(2,1)S(1)} %constant_dynamic-slice_fusion), channel_id=1, replica_groups=mesh['ep'=16,'tp'=2] {'ep'}, dimensions={0}, use_global_device_ids=true | all-gather | bytes 557056 | tf_op jit(solution)/shard_map/all_gather | solution.py:133
  77.0 1.7 %convolution_convert_fusion.3 = bf16[256,512]{1,0:T(8,128)(2,1)S(1)} fusion(bf16[256,1024]{1,0:T(8,128)(2,1)S(1)} %all_gather.13, bf16[1024,256]{1,0:T(8,128)(2,1)} %param.31, bf16[1024,256]{1,0:T(8,128)(2,1)} %param.30), kind=kOutput, calls=%fused_computation.7 | convolution fusion | flops 270663680 | bytes 1835008 | tf_op jit(solution)/shard_map/dot_general | solution.py:132
  78.7 9.2 %all-gather = bf16[512,512]{1,0:T(8,128)(2,1)S(1)} all-gather(bf16[256,512]{1,0:T(8,128)(2,1)S(1)} %convolution_convert_fusion.3), channel_id=2, replica_groups=mesh['ep'=16,'tp'=2] {'tp'}, dimensions={0}, use_global_device_ids=true | all-gather | bytes 786432 | tf_op jit(solution)/shard_map/all_gather | solution.py:138
  87.9 0.1 reduce_sum.85
  88.0 0.1 convert_element_type.94
  88.1 0.0 copy-start.4
  88.1 1.3 fusion.33
  89.4 0.0 reduce-scatter.2.cloned.1.call-update
  89.4 0.0 all-to-all-done
  89.5 0.2 copy.61
  89.7 11.2 %all_gather.12 = bf16[16,12,2048]{2,0,1:T(8,128)(2,1)S(1)} all-gather(bf16[16,12,1024]{2,0,1:T(8,128)(2,1)S(1)} %copy.61), channel_id=1, replica_groups=mesh['ep'=16,'tp'=2] {'tp'}, dimensions={2}, use_global_device_ids=true | all-gather | bytes 1179648 | tf_op jit(solution)/shard_map/all_gather | solution.py:107
  100.9 0.0 copy-done.4
  100.9 1.1 convolution_bitcast_fusion.1
  101.9 2.3 %convolution_convert_fusion = bf16[16,12,2048]{2,0,1:T(8,128)(2,1)S(1)} fusion(bf16[1,256,2048]{2,1,0:T(8,128)(2,1)S(1)} %copy-done, bf16[16,12,2048]{2,0,1:T(8,128)(2,1)S(1)} %all_gather.12, bf16[1,2048,256]{2,1,0:T(8,128)(2,1)} %param.36, f32[16,1,12,256]{3,0,2,1:T(8,128)} %convolution_bitcast_fusion.1), kind=kOutput, calls=%fused_computation | convolution fusion | flops 403341312 | bytes 3866624 | tf_op jit(solution)/shard_map/skcw,kwd->skcd/dot_general | solution.py:115
  104.2 0.1 copy.77
  104.3 0.0 copy-start.11
  104.3 0.0 copy-start.9
  104.3 12.4 %all_to_all.15 = bf16[16,1,12,2,1024]{4,0,2,1,3:T(8,128)(2,1)S(1)} all-to-all(bf16[16,1,12,2,1024]{4,0,2,1,3:T(8,128)(2,1)S(1)} %bitcast.83), channel_id=1, replica_groups=mesh['ep'=16,'tp'=2] {'tp'}, dimensions={3} | all-to-all | bytes 1572864 | tf_op jit(solution)/shard_map/all_to_all | solution.py:121
  116.7 0.2 reduce_sum.84
  116.9 1.0 copy.64
  118.0 3.6 %all-to-all-start.2 = ((bf16[16,12,1024]{2,1,0:T(8,128)(2,1)}), bf16[16,12,1024]{2,1,0:T(8,128)(2,1)S(1)}, u32[]{:S(2)}, u32[]{:S(2)}) async-start(bf16[16,12,1024]{2,1,0:T(8,128)(2,1)} %copy.64), calls=%async_computation.2 | async-start | bytes 1048576 | tf_op jit(solution)/shard_map/all_to_all | solution.py:124
  121.6 0.1 select_reduce_fusion
  121.7 0.1 fusion.12
  121.8 14.3 %all-to-all-done.2 = bf16[16,12,1024]{2,1,0:T(8,128)(2,1)S(1)} async-done(((bf16[16,12,1024]{2,1,0:T(8,128)(2,1)}), bf16[16,12,1024]{2,1,0:T(8,128)(2,1)S(1)}, u32[]{:S(2)}, u32[]{:S(2)}) %all-to-all-start.2) | async-done | bytes 393248 | tf_op jit(solution)/shard_map/all_to_all | solution.py:124
  136.1 0.1 reshape.161
  136.2 11.1 %reduce-scatter.2.cloned.1.call-done = f32[16,1024]{1,0:T(8,128)} async-done(((f32[256,1024]{1,0:T(8,128)}), f32[16,1024]{1,0:T(8,128)}) %reduce-scatter.2.cloned.1.call-update) | async-done | bytes 65552 | tf_op jit(solution)/shard_map/reduce_scatter | solution.py:143
  147.3 1.7 %fusion.8 = bf16[16,1024]{1,0:T(8,128)(2,1)} fusion(f32[192,16]{0,1:T(8,128)S(1)} %select_reduce_fusion, bf16[192,1024]{1,0:T(8,128)(2,1)S(1)} %reshape.161, f32[16,1024]{1,0:T(8,128)} %reduce-scatter.2.cloned.1.call-done, f32[16,2048]{1,0:T(8,128)S(1)} %copy-done.6, s32[]{:T(128)S(6)} %select_n.8, f32[16]{0:T(128)S(1)} %fusion.12), kind=kOutput, calls=%fused_computation.15 | convolution fusion | flops 37814272 | bytes 569412 | tf_op jit(solution)/shard_map/dot_general | solution.py:125
  (26 shorter events, 0.2 us)
Async XLA Ops:
  6.5 95.4 %copy-start = (bf16[1,256,2048]{2,1,0:T(8,128)(2,1)S(1)}, bf16[1,256,2048]{2,1,0:T(8,128)(2,1)}, u32[]{:S(2)}) copy-start(bf16[1,256,2048]{2,1,0:T(8,128)(2,1)} %param.37) | copy-start | bytes 3145732
  6.5 5.1 %copy-start.1 = (bf16[16,2048]{1,0:T(8,128)(2,1)S(1)}, bf16[16,2048]{1,0:T(8,128)(2,1)}, u32[]{:S(2)}) copy-start(bf16[16,2048]{1,0:T(8,128)(2,1)} %param.20) | copy-start | bytes 196612
  6.5 5.1 %copy-start.7 = (f32[2048]{0:T(1024)S(1)}, f32[2048]{0:T(1024)}, u32[]{:S(2)}) copy-start(f32[2048]{0:T(1024)} %param.23) | copy-start | bytes 24580
  6.5 7.1 %copy-start.2 = (f32[16,2,128,128]{3,2,1,0:T(8,128)S(1)}, f32[16,2,128,128]{3,2,1,0:T(8,128)}, u32[]{:S(2)}) copy-start(f32[16,2,128,128]{3,2,1,0:T(8,128)} %param.22) | copy-start | bytes 6291460
  6.5 34.1 %all-reduce.2.cloned.1.call-start = ((), (), s32[]{:S(2)}) async-start(), calls=%async_computation.4 | async-start | bytes 131072 | tf_op jit(solution)/shard_map/psum | solution.py:81
  13.2 3.7 %copy-start.8 = (s32[16,6]{0,1:T(8,128)S(1)}, s32[16,6]{0,1:T(8,128)}, u32[]{:S(2)}) copy-start(s32[16,6]{0,1:T(8,128)} %param.33) | copy-start | bytes 1156
  13.2 2.7 %copy-start.3 = (bf16[256,2048]{1,0:T(8,128)(2,1)S(1)}, bf16[256,2048]{1,0:T(8,128)(2,1)}, u32[]{:S(2)}) copy-start(bf16[256,2048]{1,0:T(8,128)(2,1)} %param.27) | copy-start | bytes 3145732
  13.4 28.9 %copy-start.10 = (f32[2048]{0:T(1024)S(1)}, f32[2048]{0:T(1024)}, u32[]{:S(2)}) copy-start(f32[2048]{0:T(1024)} %param.28) | copy-start | bytes 24580
  44.5 45.0 %all-to-all-start = ((bf16[16,12,1024]{2,1,0:T(8,128)(2,1)}), bf16[16,12,1024]{2,1,0:T(8,128)(2,1)S(1)}, u32[]{:S(2)}, u32[]{:S(2)}) async-start(bf16[16,12,1024]{2,1,0:T(8,128)(2,1)} %reshape.155), calls=%async_computation | async-start | bytes 1048576 | tf_op jit(solution)/shard_map/all_to_all | solution.py:106
  50.1 97.2 %reduce-scatter.2.cloned.1.call-start = ((), (), s32[]{:S(2)}) async-start(), calls=%async_computation.5 | async-start | bytes 1114112 | tf_op jit(solution)/shard_map/reduce_scatter | solution.py:143
  77.0 11.1 %copy-start.5 = (bf16[256,1024]{1,0:T(8,128)(2,1)S(1)}, bf16[256,1024]{1,0:T(8,128)(2,1)}, u32[]{:S(2)}) copy-start(bf16[256,1024]{1,0:T(8,128)(2,1)} %param.32) | copy-start | bytes 1572868
  88.1 12.8 %copy-start.4 = (bf16[1,2048,256]{2,1,0:T(8,128)(2,1)S(1)}, bf16[1,2048,256]{2,1,0:T(8,128)(2,1)}, u32[]{:S(2)}) copy-start(bf16[1,2048,256]{2,1,0:T(8,128)(2,1)} %param.35) | copy-start | bytes 3145732
  104.3 17.2 %copy-start.11 = (bf16[2048]{0:T(1024)(128)(2,1)S(1)}, bf16[2048]{0:T(1024)(128)(2,1)}, u32[]{:S(2)}) copy-start(bf16[2048]{0:T(1024)(128)(2,1)} %param.29) | copy-start | bytes 12292
  104.3 17.3 %copy-start.9 = (f32[16,6]{0,1:T(8,128)S(1)}, f32[16,6]{0,1:T(8,128)}, u32[]{:S(2)}) copy-start(f32[16,6]{0,1:T(8,128)} %param.34) | copy-start | bytes 1156
  116.7 30.6 %copy-start.6 = (f32[16,2048]{1,0:T(8,128)S(1)}, f32[16,2048]{1,0:T(8,128)}, u32[]{:S(2)}) copy-start(f32[16,2048]{1,0:T(8,128)} %get-tuple-element.6) | copy-start | bytes 393220
  118.0 18.2 %all-to-all-start.2 = ((bf16[16,12,1024]{2,1,0:T(8,128)(2,1)}), bf16[16,12,1024]{2,1,0:T(8,128)(2,1)S(1)}, u32[]{:S(2)}, u32[]{:S(2)}) async-start(bf16[16,12,1024]{2,1,0:T(8,128)(2,1)} %copy.64), calls=%async_computation.2 | async-start | bytes 1048576 | tf_op jit(solution)/shard_map/all_to_all | solution.py:124
Sparse Core Ops, SparseCore 0:
  17.0 23.6 all-reduce.1
  89.6 57.7 reduce-scatter.1
